TPU v7x, 32 devices: a whole 2x2x4 slice. The times are simulated.
32 devices in a mesh: rep: 4 (over z), fs: 4 (over y, x), tp: 2 (over core).
Axes of the slice: x: 2, y: 2, z: 4, core: 2. Of those that a mesh axis runs over, the one named last changes fastest.
Arguments:
- hidden_pre: bfloat16 [8192, 4096], P(('rep', 'fs'), 'tp'), may hold values from -6 to 6
- out_grad: bfloat16 [8192, 2048], P(('rep', 'fs')), may hold values from -8 to 8
- down_weight: bfloat16 [2048, 4096], P('fs', 'tp'), may hold values from -0.09375 to 0.09375
Outputs:
- hidden_grad: bfloat16 [8192, 4096], P(('rep', 'fs'), 'tp')
- weight_grad: float32 [2048, 4096], P('fs', 'tp')
All inputs are finite; a program needn't handle non-finite values.
Results may differ from a plain program's by a relative error of at most 0.0049.
Values may be sent and summed in bfloat16 or wider, within the bound.
A program may use at most 64 MiB of HBM per device.

v0:
```python
import math

import jax
import jax.numpy as jnp
from jax import lax
from jax.sharding import PartitionSpec as P


def body(hidden_pre, out_grad, down_weight):
    rows = hidden_pre.shape[0]
    ff_local = hidden_pre.shape[1]
    back = jnp.dot(
        out_grad,
        lax.all_gather(down_weight, "fs", axis=0, tiled=True),
        preferred_element_type=jnp.float32,
    )
    positive = jnp.maximum(hidden_pre.astype(jnp.float32), 0.0)
    hidden_grad = (2.0 * positive * back).astype(jnp.bfloat16)
    act = (positive * positive).astype(jnp.bfloat16)
    partial_value = lax.dot_general(
        out_grad, act, (((0,), (0,)), ((), ())), preferred_element_type=jnp.float32
    )
    partial_value = partial_value.astype(jnp.bfloat16)
    received = lax.all_to_all(partial_value, "fs", split_axis=0, concat_axis=0, tiled=True)
    groups = lax.axis_size("fs")
    local_sum = jnp.sum(
        received.reshape(groups, received.shape[0] // groups, ff_local), axis=0, dtype=jnp.float32
    )
    total = lax.psum(local_sum, "rep")
    tokens_all = rows * lax.axis_size("rep") * groups
    weight_grad = total * (1.0 / math.sqrt(tokens_all))
    return (hidden_grad, weight_grad)


def solution(mesh):
    placed = (P(("rep", "fs"), "tp"), P(("rep", "fs"), None), P("fs", "tp"))
    return jax.shard_map(
        body,
        mesh=mesh,
        in_specs=placed,
        out_specs=(P(("rep", "fs"), "tp"), P("fs", "tp")),
        check_vma=False,
    )
```

profile of v0, /device:TPU:0, one launch (start us, length us, event | category | flops | bytes accessed | tf_op | source)
XLA Modules:
  0.0 297.2 jit_solution(1170586137731124309)
XLA Ops:
  8.0 0.0 copy-start
  8.0 0.0 all-reduce.2.cloned.1.call-start
  8.1 1.5 copy-done
  9.6 8.3 %convolution_convert_fusion = bf16[2048,2048]{0,1:T(8,128)(2,1)} fusion(bf16[512,2048]{1,0:T(8,128)(2,1)S(1)} %copy-done, bf16[512,2048]{1,0:T(8,128)(2,1)} %param.3), kind=kOutput, calls=%fused_computation.1 | convolution fusion | flops 4303355904 | bytes 12582912 | tf_op jit(solution)/shard_map/dot_general | solution.py:20
  17.9 98.5 %all_to_all.9 = bf16[4,512,2048]{2,1,0:T(8,128)(2,1)S(1)} all-to-all(bf16[4,512,2048]{2,1,0:T(8,128)(2,1)} %bitcast.6), channel_id=1, replica_groups=mesh['rep'=4,'fs'=4,'tp'=2] {'fs'}, dimensions={0} | all-to-all | bytes 16777216 | tf_op jit(solution)/shard_map/all_to_all | solution.py:24
  116.4 3.9 %convert_reduce_fusion = f32[512,2048]{1,0:T(8,128)} fusion(bf16[4,512,2048]{2,1,0:T(8,128)(2,1)S(1)} %all_to_all.9), kind=kLoop, calls=%fused_computation | loop fusion | flops 7340032 | bytes 12582912 | tf_op jit(solution)/shard_map/reduce_sum | solution.py:26
  120.3 0.0 all-reduce.2.cloned.1.call-update
  120.3 0.0 all-gather.2.cloned.1.call-start
  120.4 0.5 all-gather.2.cloned.1.call-update
  120.9 154.4 %all-reduce.2.cloned.1.call-done = f32[512,2048]{1,0:T(8,128)} async-done(((f32[512,2048]{1,0:T(8,128)}), f32[512,2048]{1,0:T(8,128)}) %all-reduce.2.cloned.1.call-update) | async-done | bytes 4194320 | tf_op jit(solution)/shard_map/psum | solution.py:29
  275.4 5.0 %broadcast_multiply_fusion = f32[512,2048]{1,0:T(8,128)} fusion(f32[512,2048]{1,0:T(8,128)} %all-reduce.2.cloned.1.call-done), kind=kLoop, calls=%fused_computation.5 | loop fusion | flops 1048576 | bytes 8388608 | tf_op jit(solution)/shard_map/mul | solution.py:31
  280.3 0.0 all-gather.2.cloned.1.call-done
  280.3 9.5 %multiply_convert_fusion.1 = bf16[512,2048]{1,0:T(8,128)(2,1)} fusion(bf16[512,2048]{1,0:T(8,128)(2,1)} %param.3, bf16[512,2048]{1,0:T(8,128)(2,1)S(1)} %copy-done, bf16[2048,2048]{1,0:T(8,128)(2,1)} %all-gather.2.cloned.1.call-done), kind=kOutput, calls=%fused_computation.3 | convolution fusion | flops 4300210176 | bytes 14680064 | tf_op jit(solution)/shard_map/dot_general | solution.py:12
Async XLA Ops:
  8.0 1.6 copy-start
  8.0 267.3 %all-reduce.2.cloned.1.call-start = ((), (), s32[]{:S(2)}) async-start(), calls=%async_computation.2 | async-start | bytes 8388608 | tf_op jit(solution)/shard_map/psum | solution.py:29
  120.3 160.0 %all-gather.2.cloned.1.call-start = ((), (), s32[]{:S(2)}) async-start(), calls=%async_computation.1 | async-start | bytes 10485760 | tf_op jit(solution)/shard_map/all_gather | solution.py:14
Sparse Core Ops, SparseCore 0:
  120.4 154.8 all-reduce.1
Sparse Core Ops, SparseCore 1:
  122.7 87.2 all-gather.1
where the time goes:
time: 297 us
  waiting for transfers between devices  155 us (52%)
  blocking collectives  98.5 us (33%)
  matrix products  17.8 us (6%)
  between operations  15.5 us (5%)
  other arithmetic  8.83 us (3%)
    psum x1, waiting for transfers between devices, body(): total = lax.psum(local_sum, 'rep')  154 us
    all_to_all x1, blocking collectives, body(): lax.all_to_all(partial_value, 'fs', split_axis=0, concat_axis=0, tiled=True)  98.5 us
    dot_general x1, matrix products, body(): jnp.dot(out_grad, lax.all_gather(down_weight, 'fs', axis=0, tiled=True),...  9.45 us
    dot_general x1, matrix products, body(): lax.dot_general(out_grad, act, (((0,), (0,)), ((), ())), preferred_elemen...  8.35 us
  transfers between devices with their start and end apart: 2, of which 1 were waited for; matrix products, arithmetic and copies ran while one was open for 2% of the time, Pallas kernels for 0%

commit v1 on v0

v1 whole, which is shorter than its diff:
```python
import functools
import math

import jax
import jax.numpy as jnp
from jax import lax
from jax.experimental import pallas as pl
from jax.experimental.pallas import tpu as pltpu
from jax.sharding import PartitionSpec as P

MESH = pl.DeviceIdType.MESH
BF = jnp.bfloat16
F32 = jnp.float32


def plain_body(hidden_pre, out_grad, down_weight):
    rows = hidden_pre.shape[0]
    ff_local = hidden_pre.shape[1]
    back = jnp.dot(
        out_grad,
        lax.all_gather(down_weight, "fs", axis=0, tiled=True),
        preferred_element_type=F32,
    )
    positive = jnp.maximum(hidden_pre.astype(F32), 0.0)
    hidden_grad = (2.0 * positive * back).astype(BF)
    act = (positive * positive).astype(BF)
    partial_value = lax.dot_general(
        out_grad, act, (((0,), (0,)), ((), ())), preferred_element_type=F32
    )
    partial_value = partial_value.astype(BF)
    received = lax.all_to_all(partial_value, "fs", split_axis=0, concat_axis=0, tiled=True)
    groups = lax.axis_size("fs")
    local_sum = jnp.sum(
        received.reshape(groups, received.shape[0] // groups, ff_local), axis=0, dtype=F32
    )
    total = lax.psum(local_sum, "rep")
    tokens_all = rows * lax.axis_size("rep") * groups
    return (hidden_grad, total * (1.0 / math.sqrt(tokens_all)))


def kernel(chunks, hp, og, w, hg_out, tot_out,
           ogcat, ogt, whalf, hpc, pbs, pbr, pbo, gs, gr, gown, zs, z1r, z2r, zt, hg,
           l_og, l_w, l_hp, o_hg, o_t,
           og_s, og_r, od_s, od_r, w_s, w_r, hp_s, hp_r, pb_s, pb_r, g_s, g_r,
           z1_s, z1_rs, z2_s, z2_rs, z3_s, z3_rs):
    rows, ff = hp.shape
    depth = w.shape[0]
    half = 2 * depth
    fc = ff // chunks
    part = rows // 2
    fs = lax.axis_index("fs")
    core = lax.axis_index("tp")
    z = lax.axis_index("rep")
    last = lax.axis_size("rep") - 1
    a, b = fs // 2, fs % 2
    apeer = {"fs": (1 - a) * 2 + b}
    bpeer = {"fs": a * 2 + (1 - b)}
    cpeer = {"tp": 1 - core}
    znext = {"rep": z + 1 - 2 * (z % 2)}
    zmid = {"rep": last - z}
    outer = jnp.logical_or(z == 0, z == last)
    inner = jnp.logical_not(outer)

    def remote(src, dst, ssem, rsem, peer):
        return pltpu.make_async_remote_copy(
            src_ref=src, dst_ref=dst, send_sem=ssem, recv_sem=rsem,
            device_id=peer, device_id_type=MESH)

    def cols(c):
        return pl.ds(pl.multiple_of(c * fc, fc), fc)

    mine = pl.ds(pl.multiple_of(b * depth, depth), depth)
    theirs = pl.ds(pl.multiple_of((1 - b) * depth, depth), depth)
    low = pl.ds(pl.multiple_of(core * part, part), part)
    mid = pl.ds(pl.multiple_of(rows + core * part, part), part)
    mid_other = pl.ds(pl.multiple_of(rows + (1 - core) * part, part), part)

    def load_og():
        return pltpu.make_async_copy(
            og.at[:, pl.ds(pl.multiple_of(a * half, half), half)], ogcat.at[pl.ds(0, rows)], l_og)

    def load_w(c):
        return pltpu.make_async_copy(w.at[:, cols(c)], whalf.at[c, mine], l_w.at[c])

    def load_hp(c):
        return pltpu.make_async_copy(hp.at[:, cols(c)], hpc.at[0, c], l_hp.at[c])

    def store_hg(c):
        return pltpu.make_async_copy(hg.at[c], hg_out.at[:, cols(c)], o_hg.at[c])

    def store_tot(c):
        return pltpu.make_async_copy(zt.at[c], tot_out.at[:, cols(c)], o_t.at[c])

    def send_og():
        return remote(og.at[low, pl.ds(pl.multiple_of((1 - a) * half, half), half)],
                      ogcat.at[mid], og_s, og_r, apeer)

    def send_od():
        return remote(ogcat.at[mid], ogcat.at[mid], od_s, od_r, cpeer)

    def recv_od():
        return remote(ogcat.at[mid_other], ogcat.at[mid_other], od_s, od_r, cpeer)

    def send_w(c):
        return remote(w.at[:, cols(c)], whalf.at[c, mine], w_s.at[c], w_r.at[c], bpeer)

    def recv_w(c):
        return remote(w.at[:, cols(c)], whalf.at[c, theirs], w_s.at[c], w_r.at[c], bpeer)

    def send_hp(c):
        return remote(hp.at[:, cols(c)], hpc.at[1, c], hp_s.at[c], hp_r.at[c], apeer)

    def send_pb(c):
        return remote(pbs.at[c], pbr.at[c], pb_s.at[c], pb_r.at[c], apeer)

    def send_g(c):
        return remote(gs.at[c], gr.at[c], g_s.at[c], g_r.at[c], bpeer)

    def send_z1(c):
        return remote(zs.at[c], z1r.at[c], z1_s.at[c], z1_rs.at[c], znext)

    def send_z2(c):
        return remote(zs.at[c], z2r.at[c], z2_s.at[c], z2_rs.at[c], zmid)

    def send_z3(c):
        return remote(zt.at[c], zt.at[c], z3_s.at[c], z3_rs.at[c], znext)

    barrier = pltpu.get_barrier_semaphore()
    for peer in (apeer, bpeer, cpeer, znext, zmid):
        pl.semaphore_signal(barrier, inc=1, device_id=peer, device_id_type=MESH)
    load_og().start()
    pl.semaphore_wait(barrier, 5)

    send_og().start()

    @pl.loop(0, chunks)
    def _(c):
        send_w(c).start()
        send_hp(c).start()
        load_w(c).start()
        load_hp(c).start()

    load_og().wait()
    ogt[:, 0:rows] = ogcat[0:rows, :].T
    send_og().wait_recv()
    send_od().start()
    recv_od().wait_recv()
    ogt[:, rows:2 * rows] = ogcat[rows:2 * rows, :].T

    @pl.loop(0, chunks)
    def _(c):
        load_w(c).wait()
        recv_w(c).wait_recv()
        pbs[c] = jnp.dot(ogcat[rows:2 * rows, :], whalf[c], preferred_element_type=F32).astype(BF)
        send_pb(c).start()
        pbo[c] = jnp.dot(ogcat[0:rows, :], whalf[c], preferred_element_type=F32)
        load_hp(c).wait()
        send_hp(c).wait_recv()
        positive = jnp.maximum(hpc[:, c].reshape(2 * rows, fc).astype(F32), 0.0)
        act = (positive * positive).astype(BF)
        gs[c] = jnp.dot(ogt[theirs, :], act, preferred_element_type=F32).astype(BF)
        send_g(c).start()
        gown[c] = jnp.dot(ogt[mine, :], act, preferred_element_type=F32)

    @pl.loop(0, chunks + 4)
    def _(i):
        @pl.when(i < chunks)
        def _():
            send_g(i).wait_recv()

            @pl.when(outer)
            def _():
                zs[i] = (gown[i] + gr[i].astype(F32)).astype(BF)
                send_z1(i).start()

        @pl.when(jnp.logical_and(inner, jnp.logical_and(i >= 1, i < chunks + 1)))
        def _():
            c = i - 1
            send_z1(c).wait_recv()
            zs[c] = (gown[c] + gr[c].astype(F32) + z1r[c].astype(F32)).astype(BF)
            send_z2(c).start()

        @pl.when(jnp.logical_and(inner, jnp.logical_and(i >= 2, i < chunks + 2)))
        def _():
            c = i - 2
            send_z2(c).wait_recv()
            zt[c] = (zs[c].astype(F32) + z2r[c].astype(F32)).astype(BF)
            send_z3(c).start()
            store_tot(c).start()

        @pl.when(jnp.logical_and(i >= 3, i < chunks + 3))
        def _():
            c = i - 3
            send_pb(c).wait_recv()
            positive = jnp.maximum(hpc[0, c].astype(F32), 0.0)
            hg[c] = (2.0 * positive * (pbo[c] + pbr[c].astype(F32))).astype(BF)
            store_hg(c).start()

        @pl.when(jnp.logical_and(outer, i >= 4))
        def _():
            c = i - 4
            send_z3(c).wait_recv()
            store_tot(c).start()

    send_og().wait_send()
    send_od().wait_send()

    @pl.loop(0, chunks)
    def _(c):
        send_w(c).wait_send()
        send_hp(c).wait_send()
        send_pb(c).wait_send()
        send_g(c).wait_send()
        store_hg(c).wait()
        store_tot(c).wait()

        @pl.when(outer)
        def _():
            send_z1(c).wait_send()

        @pl.when(inner)
        def _():
            send_z2(c).wait_send()
            send_z3(c).wait_send()


def paired_body(hidden_pre, out_grad, down_weight):
    rows, ff = hidden_pre.shape
    depth = down_weight.shape[0]
    chunks = max(1, ff // 256)
    fc = ff // chunks
    any_spec = pl.BlockSpec(memory_space=pl.ANY)

    def block(r, dtype):
        return pltpu.VMEM((chunks, r, fc), dtype)

    sem = pltpu.SemaphoreType.DMA
    hidden_grad, total = pl.pallas_call(
        functools.partial(kernel, chunks),
        out_shape=(jax.ShapeDtypeStruct((rows, ff), BF), jax.ShapeDtypeStruct((depth, ff), BF)),
        in_specs=[any_spec] * 3,
        out_specs=(any_spec, any_spec),
        scratch_shapes=[
            pltpu.VMEM((2 * rows, 2 * depth), BF),
            pltpu.VMEM((2 * depth, 2 * rows), BF),
            block(2 * depth, BF),
            pltpu.VMEM((2, chunks, rows, fc), BF),
            block(rows, BF), block(rows, BF), block(rows, F32),
            block(depth, BF), block(depth, BF), block(depth, F32),
            block(depth, BF), block(depth, BF), block(depth, BF), block(depth, BF),
            block(rows, BF),
            sem, sem((chunks,)), sem((chunks,)), sem((chunks,)), sem((chunks,)),
            sem, sem, sem, sem,
        ] + [sem((chunks,))] * 14,
        compiler_params=pltpu.CompilerParams(
            collective_id=0, has_side_effects=True, vmem_limit_bytes=60 * 1024 * 1024
        ),
    )(hidden_pre, out_grad, down_weight)
    tokens_all = rows * lax.axis_size("rep") * lax.axis_size("fs")
    return hidden_grad, total.astype(F32) * (1.0 / math.sqrt(tokens_all))


def solution(mesh):
    placed = (P(("rep", "fs"), "tp"), P(("rep", "fs"), None), P("fs", "tp"))
    two_by_two = mesh.shape["fs"] == 4 and mesh.shape["tp"] == 2 and mesh.shape["rep"] == 4
    return jax.shard_map(
        paired_body if two_by_two else plain_body,
        mesh=mesh,
        in_specs=placed,
        out_specs=(P(("rep", "fs"), "tp"), P("fs", "tp")),
        check_vma=False,
    )
```

time: 297 us -> 133 us (0.45)
  waiting for transfers between devices: 155 us -> 0 us
  Pallas kernels: 0 us -> 127 us
  blocking collectives: 98.5 us -> 0 us
  matrix products: 17.8 us -> 0 us
  between operations: 15.5 us -> 0.65 us
  other arithmetic: 8.83 us -> 4.32 us
    psum x1 -> x0, waiting for transfers between devices: 154 us -> none  [body(): total = lax.psum(local_sum, 'rep')]
    pallas_call x0 -> x1, Pallas kernels: none -> 127 us  [paired_body(): pl.pallas_call(functools.partial(kernel, chunks), out_shape=(jax.ShapeDty...]
    all_to_all x1 -> x0, blocking collectives: 98.5 us -> none  [body(): lax.all_to_all(partial_value, 'fs', split_axis=0, concat_axis=0, tiled=True)]
    dot_general x2 -> x0, matrix products: 17.8 us -> none  [the longest x1 9.45 us: body(): jnp.dot(out_grad, lax.all_gather(down_weight, 'fs', axis=0, tiled=True),...]
    reduce_sum x1 -> x0, other arithmetic: 3.88 us -> none  [body(): jnp.sum(received.reshape(groups, received.shape[0] // groups, ff_local),...]
  transfers between devices with their start and end apart: 2 -> 0, of which waited for: 1 -> 0; matrix products, arithmetic and copies ran while one was open for 2% -> 0% of each run, Pallas kernels for 0% -> 0%
where the time goes in v1:
time: 133 us
  Pallas kernels  127 us (95%)
  other arithmetic  4.32 us (3%)
    pallas_call x1, Pallas kernels, paired_body(): pl.pallas_call(functools.partial(kernel, chunks), out_shape=(jax.ShapeDty...  127 us
    mul x1, other arithmetic, paired_body(): return (hidden_grad, total.astype(F32) * (1.0 / math.sqrt(tokens_all)))  4.32 us

profile of v1, /device:TPU:0, one launch (start us, length us, event | category | flops | bytes accessed | tf_op | source)
XLA Modules:
  0.0 133.2 jit_solution(9460832868013119824)
XLA Ops:
  0.6 126.9 %shard_map.50 = (bf16[512,2048]{1,0:T(8,128)(2,1)}, bf16[512,2048]{1,0:T(8,128)(2,1)}) custom-call(bf16[512,2048]{1,0:T(8,128)(2,1)} %hp.1, bf16[512,2048]{1,0:T(8,128)(2,1)} %og.1, bf16[512,2048]{1,0:T(8,128)(2,1)} %w.1), custom_call_target="tpu_custom_call" | custom-call | tf_op jit(solution)/shard_map/pallas_call | solution.py:238
  127.6 0.0 copy-start
  127.6 4.3 %convert_multiply_fusion = f32[512,2048]{1,0:T(8,128)} fusion(bf16[512,2048]{1,0:T(8,128)(2,1)} %get-tuple-element.5), kind=kLoop, calls=%fused_computation | loop fusion | flops 2097152 | bytes 6291456 | tf_op jit(solution)/shard_map/mul | solution.py:260
  131.9 0.0 copy-done
  131.9 1.3 copy.6
Async XLA Ops:
  127.6 4.3 %copy-start = (bf16[512,2048]{1,0:T(8,128)(2,1)S(1)}, bf16[512,2048]{1,0:T(8,128)(2,1)}, u32[]{:S(2)}) copy-start(bf16[512,2048]{1,0:T(8,128)(2,1)} %get-tuple-element.8) | copy-start | bytes 6291460

commit v2 on v0

v2 whole, which is shorter than its diff:
```python
import math

import jax
import jax.numpy as jnp
from jax import lax
from jax.experimental import pallas as pl
from jax.experimental.pallas import tpu as pltpu
from jax.sharding import PartitionSpec as P

MESH = pl.DeviceIdType.MESH
BF = jnp.bfloat16
F32 = jnp.float32


def plain_body(hidden_pre, out_grad, down_weight):
    rows = hidden_pre.shape[0]
    ff_local = hidden_pre.shape[1]
    back = jnp.dot(
        out_grad,
        lax.all_gather(down_weight, "fs", axis=0, tiled=True),
        preferred_element_type=F32,
    )
    positive = jnp.maximum(hidden_pre.astype(F32), 0.0)
    hidden_grad = (2.0 * positive * back).astype(BF)
    act = (positive * positive).astype(BF)
    partial_value = lax.dot_general(
        out_grad, act, (((0,), (0,)), ((), ())), preferred_element_type=F32
    )
    partial_value = partial_value.astype(BF)
    received = lax.all_to_all(partial_value, "fs", split_axis=0, concat_axis=0, tiled=True)
    groups = lax.axis_size("fs")
    local_sum = jnp.sum(
        received.reshape(groups, received.shape[0] // groups, ff_local), axis=0, dtype=F32
    )
    total = lax.psum(local_sum, "rep")
    tokens_all = rows * lax.axis_size("rep") * groups
    return (hidden_grad, total * (1.0 / math.sqrt(tokens_all)))


STEPS = 4


def kernel(hp, og, w, hg_out, tot_out,
           ogcat, ogt, whalf, hpc, pbs, pbr, pbo, gs, gr, gown, zs, z1r, z2r, zt, hg,
           l_og, l_w, l_hp, o_hg, o_t,
           og_s, og_r, od_s, od_r, w_s, w_r, f_s, f_r, hp_s, hp_r, pb_s, pb_r, g_s, g_r,
           z1_s, z1_rs, z2_s, z2_rs, z3_s, z3_rs):
    rows, ff = hp.shape
    depth = w.shape[0]
    chunks = 2 * STEPS
    fc = ff // chunks
    part = rows // 2
    fs = lax.axis_index("fs")
    core = lax.axis_index("tp")
    z = lax.axis_index("rep")
    last = lax.axis_size("rep") - 1
    a, b = fs // 2, fs % 2
    par = z % 2
    apeer = {"fs": (1 - a) * 2 + b}
    bpeer = {"fs": a * 2 + (1 - b)}
    cpeer = {"tp": 1 - core}
    znext = {"rep": z + 1 - 2 * par}
    zmid = {"rep": last - z}
    outer = jnp.logical_or(z == 0, z == last)
    inner = jnp.logical_not(outer)
    token_peer = (apeer, bpeer)
    weight_peer = (bpeer, apeer)

    def remote(src, dst, ssem, rsem, peer):
        return pltpu.make_async_remote_copy(
            src_ref=src, dst_ref=dst, send_sem=ssem, recv_sem=rsem,
            device_id=peer, device_id_type=MESH)

    def cut(i, size):
        return pl.ds(pl.multiple_of(i * size, size), size)

    place = (b, a)
    mine = [cut(place[q], depth) for q in range(2)]
    theirs = [cut(1 - place[q], depth) for q in range(2)]
    own_block = lambda q, p: 2 * a + p if q == 0 else 2 * p + b
    far_block = lambda q, p: 2 * (1 - a) + p if q == 0 else 2 * p + 1 - b
    low = cut(core, part)
    mid = pl.ds(pl.multiple_of(rows + core * part, part), part)
    mid_other = pl.ds(pl.multiple_of(rows + (1 - core) * part, part), part)
    both = [(q, p) for q in range(2) for p in range(2)]

    def load_og(q, p):
        return pltpu.make_async_copy(
            og.at[:, cut(own_block(q, p), depth)],
            ogcat.at[q, pl.ds(0, rows), pl.ds(p * depth, depth)], l_og.at[q, p])

    def load_w(c, q):
        return pltpu.make_async_copy(w.at[:, cut(c, fc)], whalf.at[c, mine[q]], l_w.at[c])

    def load_hp(c):
        return pltpu.make_async_copy(hp.at[:, cut(c, fc)], hpc.at[0, c], l_hp.at[c])

    def store_hg(c):
        return pltpu.make_async_copy(hg.at[c], hg_out.at[:, cut(c, fc)], o_hg.at[c])

    def store_tot(c):
        return pltpu.make_async_copy(zt.at[c], tot_out.at[:, cut(c, fc)], o_t.at[c])

    def send_og(q, p):
        return remote(og.at[low, cut(far_block(q, p), depth)],
                      ogcat.at[q, mid, pl.ds(p * depth, depth)],
                      og_s.at[q, p], og_r.at[q, p], token_peer[q])

    def pass_og(q, p, span):
        spot = ogcat.at[q, span, pl.ds(p * depth, depth)]
        return remote(spot, spot, od_s.at[q, p], od_r.at[q, p], cpeer)

    def send_w(c, q):
        return remote(w.at[:, cut(c, fc)], whalf.at[c, mine[q]], w_s.at[c], w_r.at[c], weight_peer[q])

    def recv_w(c, q):
        return remote(w.at[:, cut(c, fc)], whalf.at[c, theirs[q]], w_s.at[c], w_r.at[c], weight_peer[q])

    def pass_w(c, q):
        spot = whalf.at[c, theirs[q]]
        return remote(spot, spot, f_s.at[c], f_r.at[c], znext)

    def send_hp(c, q):
        return remote(hp.at[:, cut(c, fc)], hpc.at[1, c], hp_s.at[c], hp_r.at[c], token_peer[q])

    def send_pb(c, q):
        return remote(pbs.at[c], pbr.at[c], pb_s.at[c], pb_r.at[c], token_peer[q])

    def send_g(c, q):
        return remote(gs.at[c], gr.at[c], g_s.at[c], g_r.at[c], weight_peer[q])

    def send_z1(c):
        return remote(zs.at[c], z1r.at[c], z1_s.at[c], z1_rs.at[c], znext)

    def send_z2(c):
        return remote(zs.at[c], z2r.at[c], z2_s.at[c], z2_rs.at[c], zmid)

    def send_z3(c):
        return remote(zt.at[c], zt.at[c], z3_s.at[c], z3_rs.at[c], znext)

    def kept(j, q):
        return 2 * (2 * j + par) + q

    def passed(j, q):
        return 2 * (2 * j + 1 - par) + q

    def g_step(s):
        for q in range(2):
            c = 2 * s + q
            load_hp(c).wait()
            send_hp(c, q).wait_recv()
            if s + 2 < STEPS:
                send_hp(c + 4, q).start()
            positive = jnp.maximum(hpc[:, c].reshape(2 * rows, fc).astype(F32), 0.0)
            act = (positive * positive).astype(BF)
            gs[c] = jnp.dot(ogt[q, theirs[q], :], act, preferred_element_type=F32).astype(BF)
            send_g(c, q).start()
            gown[c] = jnp.dot(ogt[q, mine[q], :], act, preferred_element_type=F32)

    def z_a(s):
        for q in range(2):
            c = 2 * s + q
            send_g(c, q).wait_recv()

            @pl.when(outer)
            def _():
                zs[c] = (gown[c] + gr[c].astype(F32)).astype(BF)
                send_z1(c).start()

    def z_b(s):
        @pl.when(inner)
        def _():
            for q in range(2):
                c = 2 * s + q
                send_z1(c).wait_recv()
                zs[c] = (gown[c] + gr[c].astype(F32) + z1r[c].astype(F32)).astype(BF)
                send_z2(c).start()

    def z_c(s):
        @pl.when(inner)
        def _():
            for q in range(2):
                c = 2 * s + q
                send_z2(c).wait_recv()
                zt[c] = (zs[c].astype(F32) + z2r[c].astype(F32)).astype(BF)
                send_z3(c).start()
                store_tot(c).start()

    def z_d(s):
        @pl.when(outer)
        def _():
            for q in range(2):
                c = 2 * s + q
                send_z3(c).wait_recv()
                store_tot(c).start()

    def back(c, q):
        load_w(c, q).wait()
        pbs[c] = jnp.dot(ogcat[q, rows:2 * rows, :], whalf[c], preferred_element_type=F32).astype(BF)
        send_pb(c, q).start()
        pbo[c] = jnp.dot(ogcat[q, 0:rows, :], whalf[c], preferred_element_type=F32)

    def pb_direct(j):
        for which in (kept, passed):
            for q in range(2):
                recv_w(which(j, q), q).wait_recv()
                back(which(j, q), q)

    def pb_first():
        for q in range(2):
            back(kept(0, q), q)
        for q in range(2):
            pass_w(passed(0, q), q).wait_recv()
            back(passed(0, q), q)

    def finish(which, j):
        for q in range(2):
            c = which(j, q)
            send_pb(c, q).wait_recv()
            positive = jnp.maximum(hpc[0, c].astype(F32), 0.0)
            hg[c] = (2.0 * positive * (pbo[c] + pbr[c].astype(F32))).astype(BF)
            store_hg(c).start()

    barrier = pltpu.get_barrier_semaphore()
    for peer in (apeer, bpeer, cpeer, znext, zmid):
        pl.semaphore_signal(barrier, inc=1, device_id=peer, device_id_type=MESH)
    for q, p in both:
        load_og(q, p).start()
    pl.semaphore_wait(barrier, 5)
    for q, p in both:
        send_og(q, p).start()
    for q in range(2):
        send_w(kept(0, q), q).start()
    for s in range(2):
        for q in range(2):
            send_hp(2 * s + q, q).start()
    for c in range(chunks):
        load_hp(c).start()
    for c in range(chunks):
        load_w(c, c % 2).start()
    for q, p in both:
        load_og(q, p).wait()
    for q in range(2):
        ogt[q, :, 0:rows] = ogcat[q, 0:rows, :].T
    for p in range(2):
        for q in range(2):
            send_og(q, p).wait_recv()
            pass_og(q, p, mid).start()
    for q in range(2):
        for p in range(2):
            pass_og(q, p, mid_other).wait_recv()
        ogt[q, :, rows:2 * rows] = ogcat[q, rows:2 * rows, :].T

    for q in range(2):
        recv_w(kept(0, q), q).wait_recv()
        pass_w(kept(0, q), q).start()

    g_step(0)
    g_step(1)
    z_a(0)
    g_step(2)
    z_a(1)
    g_step(3)
    z_b(0)
    pb_first()
    z_a(2)
    for which in (kept, passed):
        for q in range(2):
            send_w(which(1, q), q).start()
    z_a(3)
    z_b(1)
    z_c(0)
    z_b(2)
    z_c(1)
    pb_direct(1)
    z_b(3)
    finish(kept, 0)
    finish(passed, 0)
    z_c(2)
    z_c(3)
    finish(kept, 1)
    z_d(0)
    z_d(1)
    z_d(2)
    z_d(3)
    finish(passed, 1)

    for q, p in both:
        send_og(q, p).wait_send()
        pass_og(q, p, mid).wait_send()
    for q in range(2):
        pass_w(kept(0, q), q).wait_send()
        for c in (kept(0, q), kept(1, q), passed(1, q)):
            send_w(c, q).wait_send()
    for c in range(chunks):
        send_hp(c, c % 2).wait_send()
        send_pb(c, c % 2).wait_send()
        send_g(c, c % 2).wait_send()
        store_hg(c).wait()
        store_tot(c).wait()

    @pl.when(outer)
    def _():
        for c in range(chunks):
            send_z1(c).wait_send()

    @pl.when(inner)
    def _():
        for c in range(chunks):
            send_z2(c).wait_send()
            send_z3(c).wait_send()


def paired_body(hidden_pre, out_grad, down_weight):
    rows, ff = hidden_pre.shape
    depth = down_weight.shape[0]
    chunks = 2 * STEPS
    fc = ff // chunks
    any_spec = pl.BlockSpec(memory_space=pl.ANY)

    def block(r, dtype):
        return pltpu.VMEM((chunks, r, fc), dtype)

    sem = pltpu.SemaphoreType.DMA
    hidden_grad, total = pl.pallas_call(
        kernel,
        out_shape=(jax.ShapeDtypeStruct((rows, ff), BF), jax.ShapeDtypeStruct((depth, ff), BF)),
        in_specs=[any_spec] * 3,
        out_specs=(any_spec, any_spec),
        scratch_shapes=[
            pltpu.VMEM((2, 2 * rows, 2 * depth), BF),
            pltpu.VMEM((2, 2 * depth, 2 * rows), BF),
            block(2 * depth, BF),
            pltpu.VMEM((2, chunks, rows, fc), BF),
            block(rows, BF), block(rows, BF), block(rows, F32),
            block(depth, BF), block(depth, BF), block(depth, F32),
            block(depth, BF), block(depth, BF), block(depth, BF), block(depth, BF),
            block(rows, BF),
            sem((2, 2)), sem((chunks,)), sem((chunks,)), sem((chunks,)), sem((chunks,)),
        ] + [sem((2, 2))] * 4 + [sem((chunks,))] * 16,
        compiler_params=pltpu.CompilerParams(
            collective_id=0, has_side_effects=True, vmem_limit_bytes=60 * 1024 * 1024
        ),
    )(hidden_pre, out_grad, down_weight)
    tokens_all = rows * lax.axis_size("rep") * lax.axis_size("fs")
    return hidden_grad, total.astype(F32) * (1.0 / math.sqrt(tokens_all))


def solution(mesh):
    placed = (P(("rep", "fs"), "tp"), P(("rep", "fs"), None), P("fs", "tp"))
    two_by_two = mesh.shape["fs"] == 4 and mesh.shape["tp"] == 2 and mesh.shape["rep"] == 4
    return jax.shard_map(
        paired_body if two_by_two else plain_body,
        mesh=mesh,
        in_specs=placed,
        out_specs=(P(("rep", "fs"), "tp"), P("fs", "tp")),
        check_vma=False,
    )
```

time: 297 us -> 126 us (0.42)
  waiting for transfers between devices: 155 us -> 0 us
  Pallas kernels: 0 us -> 119 us
  blocking collectives: 98.5 us -> 0 us
  matrix products: 17.8 us -> 0 us
  between operations: 15.5 us -> 0.65 us
  other arithmetic: 8.83 us -> 4.32 us
    psum x1 -> x0, waiting for transfers between devices: 154 us -> none  [body(): total = lax.psum(local_sum, 'rep')]
    pallas_call x0 -> x1, Pallas kernels: none -> 119 us  [paired_body(): pl.pallas_call(kernel, out_shape=(jax.ShapeDtypeStruct((rows, ff), BF), j...]
    all_to_all x1 -> x0, blocking collectives: 98.5 us -> none  [body(): lax.all_to_all(partial_value, 'fs', split_axis=0, concat_axis=0, tiled=True)]
    dot_general x2 -> x0, matrix products: 17.8 us -> none  [the longest x1 9.45 us: body(): jnp.dot(out_grad, lax.all_gather(down_weight, 'fs', axis=0, tiled=True),...]
    reduce_sum x1 -> x0, other arithmetic: 3.88 us -> none  [body(): jnp.sum(received.reshape(groups, received.shape[0] // groups, ff_local),...]
  transfers between devices with their start and end apart: 2 -> 0, of which waited for: 1 -> 0; matrix products, arithmetic and copies ran while one was open for 2% -> 0% of each run, Pallas kernels for 0% -> 0%
where the time goes in v2:
time: 126 us
  Pallas kernels  119 us (94%)
  other arithmetic  4.32 us (3%)
  local copies, waits for them, and re-layouts  1.32 us (1%)
    pallas_call x1, Pallas kernels, paired_body(): pl.pallas_call(kernel, out_shape=(jax.ShapeDtypeStruct((rows, ff), BF), j...  119 us
    mul x1, other arithmetic, paired_body(): return (hidden_grad, total.astype(F32) * (1.0 / math.sqrt(tokens_all)))  4.32 us

profile of v2, /device:TPU:0, one launch (start us, length us, event | category | flops | bytes accessed | tf_op | source)
XLA Modules:
  0.0 125.7 jit_solution(3548139909442299896)
XLA Ops:
  0.6 119.4 %shard_map.50 = (bf16[512,2048]{1,0:T(8,128)(2,1)}, bf16[512,2048]{1,0:T(8,128)(2,1)}) custom-call(bf16[512,2048]{1,0:T(8,128)(2,1)} %hp.1, bf16[512,2048]{1,0:T(8,128)(2,1)} %og.1, bf16[512,2048]{1,0:T(8,128)(2,1)} %w.1), custom_call_target="tpu_custom_call" | custom-call | tf_op jit(solution)/shard_map/pallas_call | solution.py:325
  120.0 0.0 copy-start
  120.1 4.3 %convert_multiply_fusion = f32[512,2048]{1,0:T(8,128)} fusion(bf16[512,2048]{1,0:T(8,128)(2,1)} %get-tuple-element.5), kind=kLoop, calls=%fused_computation | loop fusion | flops 2097152 | bytes 6291456 | tf_op jit(solution)/shard_map/mul | solution.py:346
  124.4 0.0 copy-done
  124.4 1.3 %copy.6 = bf16[512,2048]{1,0:T(8,128)(2,1)} copy(bf16[512,2048]{1,0:T(8,128)(2,1)S(1)} %copy-done) | data formatting | bytes 4194304
Async XLA Ops:
  120.0 4.3 %copy-start = (bf16[512,2048]{1,0:T(8,128)(2,1)S(1)}, bf16[512,2048]{1,0:T(8,128)(2,1)}, u32[]{:S(2)}) copy-start(bf16[512,2048]{1,0:T(8,128)(2,1)} %get-tuple-element.8) | copy-start | bytes 6291460
